TPU v7x, 32 devices: a whole 2x2x4 slice. The times are simulated.
32 devices in a mesh: grp: 2 (over y), sp: 4 (over z), tp: 4 (over x, core).
Axes of the slice: x: 2, y: 2, z: 4, core: 2. Of those that a mesh axis runs over, the one named last changes fastest.
Arguments:
- queries: bfloat16 [6144, 1024], P(('grp', 'sp'), 'tp'), parts along dimension 0, may hold values from -160 to 160
- key_rows: bfloat16 [6144, 256], P(('grp', 'sp'), 'tp'), parts along dimension 0, may hold values from -4 to 4
- value_rows: bfloat16 [6144, 256], P(('grp', 'sp'), 'tp'), parts along dimension 0, may hold values from -5 to 5
- sink_logits: float32 [16], P('tp'), may hold values from 2 to 6
- out_weight: bfloat16 [1024, 2048], replicated, may hold values from -0.75 to 0.75
- residual: bfloat16 [6144, 2048], P(('grp', 'sp', 'tp')), parts along dimension 0, may hold values from -6 to 6
- norm_gain: float32 [2048], replicated, may hold values from 0.1 to 1.9
- up_weight: bfloat16 [2048, 4096], P('sp', 'tp'), may hold values from -0.125 to 0.125
- down_weight: bfloat16 [4096, 2048], P('tp', 'sp'), may hold values from -0.09375 to 0.09375
Outputs:
- layer_out: bfloat16 [6144, 2048], P(('grp', 'sp', 'tp')), parts along dimension 0
There are 2 independent parts, one for each index of `grp`. A program takes and returns all parts, laid end to end along the dimension named above; an argument that names none is the same for every part. Nothing has to cross between parts.
All inputs are finite; a program needn't handle non-finite values.
Results may differ from a plain program's by a relative error of at most 0.017.
Values may be sent and summed in bfloat16 or wider, within the bound.
A program may use at most 64 MiB of HBM per device.

v0:
```python
import jax
import jax.numpy as jnp
from jax import lax
from jax.sharding import PartitionSpec as P

HEAD_DIM = 64
WINDOW = 128


def shifted(value, axis, steps):
    count = lax.axis_size(axis)
    leading, last = (max(0, -steps), min(count, count - steps))
    return lax.ppermute(value, axis, [(source, source + steps) for source in range(leading, last)])


def band_attend(queries, key_rows, value_rows, sink_logits, tail_keys, tail_values, offset):
    rows = queries.shape[0]
    kv_heads = key_rows.shape[1] // HEAD_DIM
    group = queries.shape[1] // (kv_heads * HEAD_DIM)
    blocks = rows // WINDOW
    all_keys = jnp.concatenate([tail_keys, key_rows], axis=0).reshape(
        blocks + 1, WINDOW, kv_heads, HEAD_DIM
    )
    all_values = jnp.concatenate([tail_values, value_rows], axis=0).reshape(
        blocks + 1, WINDOW, kv_heads, HEAD_DIM
    )
    key_blocks = jnp.concatenate([all_keys[:-1], all_keys[1:]], axis=1)
    value_blocks = jnp.concatenate([all_values[:-1], all_values[1:]], axis=1)
    query_blocks = queries.reshape(blocks, WINDOW, kv_heads, group, HEAD_DIM)
    scores = jnp.einsum(
        "nqkgd,nskd->nkgqs", query_blocks, key_blocks, preferred_element_type=jnp.float32
    ) * HEAD_DIM ** (-0.5)
    q_local = jnp.arange(WINDOW, dtype=jnp.int32) + WINDOW
    k_local = jnp.arange(2 * WINDOW, dtype=jnp.int32)
    distance = q_local[:, None] - k_local[None, :]
    key_position = (
        offset + (jnp.arange(blocks, dtype=jnp.int32)[:, None] - 1) * WINDOW + k_local[None, :]
    )
    valid = ((distance >= 0) & (distance < WINDOW))[None] & (key_position >= 0)[:, None, :]
    scores = jnp.where(valid[:, None, None], scores, -1e30)
    sink = sink_logits.reshape(kv_heads, group)[None, :, :, None, None]
    top = jnp.maximum(jnp.max(scores, axis=-1, keepdims=True), sink)
    weights = jnp.exp(scores - top)
    total = jnp.sum(weights, axis=-1, keepdims=True) + jnp.exp(sink - top)
    probs = (weights / total).astype(jnp.bfloat16)
    result = jnp.einsum(
        "nkgqs,nskd->nqkgd", probs, value_blocks, preferred_element_type=jnp.float32
    )
    return result.astype(jnp.bfloat16).reshape(rows, kv_heads * group * HEAD_DIM)


def body(
    queries,
    key_rows,
    value_rows,
    sink_logits,
    out_weight,
    residual,
    norm_gain,
    up_weight,
    down_weight,
):
    rows = queries.shape[0]
    width = key_rows.shape[1]
    kv_pair = jnp.concatenate([key_rows[rows - WINDOW :], value_rows[rows - WINDOW :]], axis=1)
    tail = shifted(kv_pair, "sp", 1)
    offset = lax.axis_index("sp") * rows
    attended = band_attend(
        queries, key_rows, value_rows, sink_logits, tail[:, :width], tail[:, width:], offset
    )
    head_cols = attended.shape[1]
    own_rows = lax.dynamic_slice_in_dim(out_weight, lax.axis_index("tp") * head_cols, head_cols, 0)
    projected = lax.psum_scatter(
        jnp.dot(attended, own_rows, preferred_element_type=jnp.float32).astype(jnp.bfloat16),
        "tp",
        scatter_dimension=0,
        tiled=True,
    ).astype(jnp.float32)
    mixed32 = (residual.astype(jnp.float32) + projected).astype(jnp.bfloat16).astype(jnp.float32)
    scale = lax.rsqrt(jnp.mean(mixed32 * mixed32, axis=-1, keepdims=True) + 1e-06)
    normed = (mixed32 * scale * norm_gain).astype(jnp.bfloat16)
    all_rows = lax.all_gather(normed, "tp", axis=0, tiled=True)
    before = jnp.dot(
        all_rows,
        lax.all_gather(up_weight, "sp", axis=0, tiled=True),
        preferred_element_type=jnp.float32,
    )
    hidden = jnp.square(jax.nn.relu(before)).astype(jnp.bfloat16)
    terms = jnp.dot(
        hidden,
        lax.all_gather(down_weight, "sp", axis=1, tiled=True),
        preferred_element_type=jnp.float32,
    )
    down = lax.psum_scatter(
        terms.astype(jnp.bfloat16), "tp", scatter_dimension=0, tiled=True
    ).astype(jnp.float32)
    return (mixed32 + down).astype(jnp.bfloat16)


def solution(mesh):
    in_specs = (
        P(("grp", "sp"), "tp"),
        P(("grp", "sp"), "tp"),
        P(("grp", "sp"), "tp"),
        P("tp"),
        P(),
        P(("grp", "sp", "tp"), None),
        P(),
        P("sp", "tp"),
        P("tp", "sp"),
    )
    out_specs = P(("grp", "sp", "tp"), None)
    return jax.shard_map(body, mesh=mesh, in_specs=in_specs, out_specs=out_specs, check_vma=False)
```

profile of v0, /device:TPU:0, one launch (start us, length us, event | category | flops | bytes accessed | tf_op | source)
XLA Modules:
  0.0 278.1 jit_solution(6048597584942686161)
XLA Ops:
  7.4 0.0 reduce-scatter.3.cloned.1.call-start
  7.4 0.7 slice.32
  8.1 0.7 slice.33
  8.8 4.9 %collective-permute-start = (bf16[128,128]{0,1:T(8,128)(2,1)S(1)}, bf16[128,128]{0,1:T(8,128)(2,1)S(1)}, u32[]{:S(2)}, u32[]{:S(2)}) collective-permute-start(bf16[128,128]{0,1:T(8,128)(2,1)S(1)} %pad_maximum_fusion.2), channel_id=1, source_target_pairs={{0,4},{4,8},{8,12},{1,5},{5,9},{9,13},{2,6},{6,10},{10,14},{3,7},{... | collective-permute-start | bytes 98312 | tf_op jit(solution)/shard_map/ppermute | solution.py:13
  13.8 0.1 add_compare_fusion
  13.9 0.3 broadcast_and_fusion
  14.2 1.0 slice.41
  15.2 1.0 slice.37
  16.3 1.8 reshape.128
  18.1 0.0 copy-start.3
  18.2 0.0 collective-permute-done
  18.2 0.9 pad_maximum_fusion
  19.1 0.1 slice.40
  19.3 0.1 slice.36
  19.5 0.7 fusion.1
  20.2 0.0 copy-done.3
  20.2 0.1 broadcast_maximum_fusion
  20.3 0.7 fusion
  21.0 0.1 exponential_add_fusion
  21.1 0.9 fusion.12
  22.0 0.3 copy.19
  22.3 4.0 %convolution_convert_fusion.1 = bf16[768,2048]{1,0:T(8,128)(2,1)} fusion(bf16[1024,2048]{1,0:T(8,128)(2,1)} %param.13, s32[]{:T(128)S(6)} %select_n.8, bf16[32,8,6,128]{3,2,1,0:T(8,128)(2,1)S(1)} %bitcast.60), kind=kOutput, calls=%fused_computation.1 | convolution fusion | flops 806879232 | bytes 4587524 | tf_op jit(solution)/shard_map/dot_general | solution.py:74
  26.3 0.0 copy-start
  26.3 0.0 copy-start.2
  26.3 0.0 reduce-scatter.3.cloned.1.call-update
  26.3 0.0 all-gather.6.cloned.1.call-start
  26.4 0.5 all-gather.6.cloned.1.call-update
  26.9 0.0 all-gather.8.cloned.1.call-start
  27.0 0.5 all-gather.8.cloned.1.call-update
  27.5 0.0 all-gather.4.cloned.1.call-start
  27.5 37.0 %reduce-scatter.3.cloned.1.call-done = bf16[192,2048]{1,0:T(8,128)(2,1)} async-done(((bf16[768,2048]{1,0:T(8,128)(2,1)}), bf16[192,2048]{1,0:T(8,128)(2,1)}) %reduce-scatter.3.cloned.1.call-update) | async-done | bytes 786448 | tf_op jit(solution)/shard_map/reduce_scatter | solution.py:73
  64.6 0.0 copy-done
  64.6 1.5 fusion.2
  66.1 0.0 copy-done.2
  66.1 2.3 fusion.4
  68.4 0.0 all-gather.4.cloned.1.call-update
  68.4 0.0 reduce-scatter.5.cloned.1.call-start
  68.5 40.8 %all-gather.6.cloned.1.call-done = bf16[2048,1024]{1,0:T(8,128)(2,1)} async-done(((bf16[512,1024]{1,0:T(8,128)(2,1)}), bf16[2048,1024]{1,0:T(8,128)(2,1)}) %all-gather.6.cloned.1.call-update) | async-done | bytes 4194320 | tf_op jit(solution)/shard_map/all_gather | solution.py:85
  109.2 80.6 %all-gather.8.cloned.1.call-done = bf16[1024,2048]{1,0:T(8,128)(2,1)} async-done(((bf16[1024,512]{1,0:T(8,128)(2,1)}), bf16[1024,2048]{1,0:T(8,128)(2,1)}) %all-gather.8.cloned.1.call-update) | async-done | bytes 4194320 | tf_op jit(solution)/shard_map/all_gather | solution.py:91
  189.8 28.3 %all-gather.4.cloned.1.call-done = bf16[768,2048]{1,0:T(8,128)(2,1)} async-done(((bf16[192,2048]{1,0:T(8,128)(2,1)}), bf16[768,2048]{1,0:T(8,128)(2,1)}) %all-gather.4.cloned.1.call-update) | async-done | bytes 3145744 | tf_op jit(solution)/shard_map/all_gather | solution.py:82
  218.1 11.9 %convolution_convert_fusion = bf16[768,2048]{1,0:T(8,128)(2,1)} fusion(bf16[1024,2048]{1,0:T(8,128)(2,1)} %all-gather.8.cloned.1.call-done, bf16[768,2048]{1,0:T(8,128)(2,1)} %all-gather.4.cloned.1.call-done, bf16[2048,1024]{1,0:T(8,128)(2,1)} %all-gather.6.cloned.1.call-done), kind=kOutput, calls=%fused_computation | convolution fusion | flops 6446383104 | bytes 14680064 | tf_op jit(solution)/shard_map/dot_general | solution.py:89
  230.0 0.0 copy-start.1
  230.0 0.0 reduce-scatter.5.cloned.1.call-update
  230.0 38.0 %reduce-scatter.5.cloned.1.call-done = bf16[192,2048]{1,0:T(8,128)(2,1)} async-done(((bf16[768,2048]{1,0:T(8,128)(2,1)}), bf16[192,2048]{1,0:T(8,128)(2,1)}) %reduce-scatter.5.cloned.1.call-update) | async-done | bytes 786448 | tf_op jit(solution)/shard_map/reduce_scatter | solution.py:94
  268.1 0.0 copy-done.1
  268.1 2.4 fusion.5
  (10 shorter events, 0.1 us)
Async XLA Ops:
  7.4 57.2 %reduce-scatter.3.cloned.1.call-start = ((), (), s32[]{:S(2)}) async-start(), calls=%async_computation.2 | async-start | bytes 3932160 | tf_op jit(solution)/shard_map/reduce_scatter | solution.py:73
  8.8 9.3 %collective-permute-start = (bf16[128,128]{0,1:T(8,128)(2,1)S(1)}, bf16[128,128]{0,1:T(8,128)(2,1)S(1)}, u32[]{:S(2)}, u32[]{:S(2)}) collective-permute-start(bf16[128,128]{0,1:T(8,128)(2,1)S(1)} %pad_maximum_fusion.2), channel_id=1, source_target_pairs={{0,4},{4,8},{8,12},{1,5},{5,9},{9,13},{2,6},{6,10},{10,14},{3,7},{... | collective-permute-start | bytes 98312 | tf_op jit(solution)/shard_map/ppermute | solution.py:13
  18.1 2.0 copy-start.3
  26.3 38.3 %copy-start = (bf16[192,2048]{1,0:T(8,128)(2,1)S(1)}, bf16[192,2048]{1,0:T(8,128)(2,1)}, u32[]{:S(2)}) copy-start(bf16[192,2048]{1,0:T(8,128)(2,1)} %param.14) | copy-start | bytes 2359300
  26.3 39.8 %copy-start.2 = (f32[2048]{0:T(1024)S(1)}, f32[2048]{0:T(1024)}, u32[]{:S(2)}) copy-start(f32[2048]{0:T(1024)} %param.15) | copy-start | bytes 24580
  26.3 82.9 %all-gather.6.cloned.1.call-start = ((), (), s32[]{:S(2)}) async-start(), calls=%async_computation.4 | async-start | bytes 5242880 | tf_op jit(solution)/shard_map/all_gather | solution.py:85
  26.9 162.9 %all-gather.8.cloned.1.call-start = ((), (), s32[]{:S(2)}) async-start(), calls=%async_computation.5 | async-start | bytes 5242880 | tf_op jit(solution)/shard_map/all_gather | solution.py:91
  27.5 190.6 %all-gather.4.cloned.1.call-start = ((), (), s32[]{:S(2)}) async-start(), calls=%async_computation.3 | async-start | bytes 3932160 | tf_op jit(solution)/shard_map/all_gather | solution.py:82
  68.4 199.7 %reduce-scatter.5.cloned.1.call-start = ((), (), s32[]{:S(2)}) async-start(), calls=%async_computation.6 | async-start | bytes 3932160 | tf_op jit(solution)/shard_map/reduce_scatter | solution.py:94
  230.0 38.1 %copy-start.1 = (bf16[192,2048]{1,0:T(8,128)(2,1)S(1)}, bf16[192,2048]{1,0:T(8,128)(2,1)}, u32[]{:S(2)}) copy-start(bf16[192,2048]{1,0:T(8,128)(2,1)} %reduce-scatter.3.cloned.1.call-done) | copy-start | bytes 2359300
Sparse Core Ops, SparseCore 0:
  26.4 38.0 reduce-scatter.2
  230.2 37.8 reduce-scatter.4
Sparse Core Ops, SparseCore 1:
  28.4 80.8 all-gather.5
  110.7 79.1 all-gather.7
  191.2 26.8 all-gather.3
where the time goes:
time: 279 us; the launch traced here: 278 us
  waiting for transfers between devices  226 us (81%)
  matrix products  17.5 us (6%)
  between operations  15.2 us (5%)
  other arithmetic  8.43 us (3%)
  local copies, waits for them, and re-layouts  5.95 us (2%)
  starting transfers between devices  5.11 us (2%)
    all_gather x1, waiting for transfers between devices, body(): lax.all_gather(down_weight, 'sp', axis=1, tiled=True)  80.6 us
    all_gather x1, waiting for transfers between devices, body(): lax.all_gather(up_weight, 'sp', axis=0, tiled=True)  40.8 us
    reduce_scatter x1, waiting for transfers between devices, body(): lax.psum_scatter(terms.astype(jnp.bfloat16), 'tp', scatter_dimension=0, t...  38 us
    reduce_scatter x1, waiting for transfers between devices, body(): lax.psum_scatter(jnp.dot(attended, own_rows, preferred_element_type=jnp.f...  37 us
    all_gather x1, waiting for transfers between devices, body(): all_rows = lax.all_gather(normed, 'tp', axis=0, tiled=True)  28.3 us
    dot_general x1, matrix products, body(): jnp.dot(hidden, lax.all_gather(down_weight, 'sp', axis=1, tiled=True), pr...  11.9 us
  transfers between devices with their start and end apart: 6, of which 5 were waited for; matrix products, arithmetic and copies ran while one was open for 3% of the time, Pallas kernels for 0%

commit v1 on v0

--- a/solution.py
+++ b/solution.py
@@ -1,6 +1,10 @@
+import functools
+
 import jax
 import jax.numpy as jnp
 from jax import lax
+from jax.experimental import pallas as pl
+from jax.experimental.pallas import tpu as pltpu
 from jax.sharding import PartitionSpec as P
 
 HEAD_DIM = 64
@@ -97,6 +101,581 @@
     return (mixed32 + down).astype(jnp.bfloat16)
 
 
+CHUNKS = 4
+F32 = jnp.float32
+BF16 = jnp.bfloat16
+
+
+def remote(src, dst, send_sem, recv_sem, device_id):
+    return pltpu.make_async_remote_copy(
+        src_ref=src,
+        dst_ref=dst,
+        send_sem=send_sem,
+        recv_sem=recv_sem,
+        device_id=device_id,
+        device_id_type=pl.DeviceIdType.MESH,
+    )
+
+
+def aligned(value, size):
+    return pl.multiple_of(value * size, size)
+
+
+def layer_kernel(
+    n,
+    queries,
+    keys,
+    values,
+    sink,
+    out_weight,
+    residual,
+    gain,
+    up,
+    down,
+    out,
+    q_buf,
+    k_buf,
+    v_buf,
+    k_wide,
+    v_wide,
+    attended,
+    att_all,
+    ow_buf,
+    res_buf,
+    mixed,
+    normed,
+    up_buf,
+    down_buf,
+    acc,
+    hidden,
+    terms,
+    pair_in,
+    chip_sum,
+    peer_in,
+    local_sem,
+    tail_send,
+    tail_recv,
+    z_send,
+    y_send,
+    w_recv,
+    att_send,
+    att_recv,
+    norm_send,
+    norm_recv,
+    pair_send,
+    pair_recv,
+    peer_send,
+    peer_recv,
+):
+    z = lax.axis_index("sp")
+    y = lax.axis_index("grp")
+    me = lax.axis_index("tp")
+    partner = me + 1 - 2 * lax.rem(me, 2)
+    across = lax.rem(me + 2, 4)
+    diagonal = lax.rem(partner + 2, 4)
+    rows, head_cols = q_buf.shape
+    own = rows // 4
+    depth = up.shape[0]
+    width = down.shape[1]
+    cols = up.shape[1]
+    wide = n * width
+    chunk = (depth // 2 // CHUNKS, down.shape[0] // 2 // CHUNKS)
+
+    barrier = pltpu.get_barrier_semaphore()
+    for step in range(1, 4):
+        pl.semaphore_signal(
+            barrier,
+            inc=1,
+            device_id={"tp": lax.rem(me + step, 4)},
+            device_id_type=pl.DeviceIdType.MESH,
+        )
+    pl.semaphore_signal(
+        barrier, inc=1, device_id={"grp": 1 - y}, device_id_type=pl.DeviceIdType.MESH
+    )
+
+    @pl.when(z > 0)
+    def _():
+        pl.semaphore_signal(
+            barrier, inc=1, device_id={"sp": z - 1}, device_id_type=pl.DeviceIdType.MESH
+        )
+
+    @pl.when(z < n - 1)
+    def _():
+        pl.semaphore_signal(
+            barrier, inc=1, device_id={"sp": z + 1}, device_id_type=pl.DeviceIdType.MESH
+        )
+
+    own_up = up_buf.at[pl.ds(aligned(z, depth), depth), :]
+    locals_ = [
+        pltpu.make_async_copy(keys, k_buf.at[pl.ds(WINDOW, rows), :], local_sem.at[0]),
+        pltpu.make_async_copy(values, v_buf.at[pl.ds(WINDOW, rows), :], local_sem.at[1]),
+        pltpu.make_async_copy(queries, q_buf, local_sem.at[2]),
+        pltpu.make_async_copy(out_weight, ow_buf, local_sem.at[3]),
+        pltpu.make_async_copy(residual, res_buf, local_sem.at[4]),
+        pltpu.make_async_copy(up, own_up, local_sem.at[5]),
+        pltpu.make_async_copy(down, down_buf.at[z], local_sem.at[6]),
+    ]
+    for copy in locals_:
+        copy.start()
+
+    edge = jnp.where(z > 0, 1, 0) + jnp.where(z < n - 1, 1, 0)
+    pl.semaphore_wait(barrier, 4 + edge)
+
+    def piece(weight, owner, half, index):
+        if weight == 0:
+            start = owner * depth + half * (depth // 2) + index * chunk[0]
+            return up_buf.at[pl.ds(pl.multiple_of(start, chunk[0]), chunk[0]), :]
+        start = half * (CHUNKS * chunk[1]) + index * chunk[1]
+        return down_buf.at[owner, pl.ds(pl.multiple_of(start, chunk[1]), chunk[1]), :]
+
+    def own_piece(weight, index):
+        start = y * (CHUNKS * chunk[weight]) + index * chunk[weight]
+        ref = up if weight == 0 else down
+        return ref.at[pl.ds(pl.multiple_of(start, chunk[weight]), chunk[weight]), :]
+
+    def z_copy(weight, owner, index, upward, source=None):
+        place = piece(weight, owner, y, index)
+        return remote(
+            place if source is None else source,
+            place,
+            z_send.at[upward, weight, owner, index],
+            w_recv.at[weight, owner, y, index],
+            {"sp": z + (1 if upward else -1)},
+        )
+
+    def y_copy(weight, owner, index):
+        place = piece(weight, owner, y, index)
+        return remote(
+            place,
+            place,
+            y_send.at[weight, owner, index],
+            w_recv.at[weight, owner, y, index],
+            {"grp": 1 - y},
+        )
+
+    def wait_piece(weight, owner, half, index):
+        place = piece(weight, owner, half, index)
+        remote(
+            place,
+            place,
+            y_send.at[weight, owner, index],
+            w_recv.at[weight, owner, half, index],
+            {"grp": 1 - y},
+        ).wait_recv()
+
+    def send_own(weight, upward):
+        for index in range(CHUNKS):
+            z_copy(weight, z, index, upward, own_piece(weight, index)).start()
+
+    def tail_copy(which):
+        source, place = ((keys, k_buf), (values, v_buf))[which]
+        return remote(
+            source.at[pl.ds(rows - WINDOW, WINDOW), :],
+            place.at[pl.ds(0, WINDOW), :],
+            tail_send.at[which],
+            tail_recv.at[which],
+            {"sp": z + 1},
+        )
+
+    @pl.when(z < n - 1)
+    def _():
+        tail_copy(0).start()
+        tail_copy(1).start()
+        send_own(0, 1)
+
+    @pl.when(z > 0)
+    def _():
+        send_own(0, 0)
+
+    def send_down(stage):
+        @pl.when((z == stage) & (z < n - 1))
+        def _():
+            send_own(1, 1)
+
+        @pl.when((n - 1 - z == stage) & (z > 0))
+        def _():
+            send_own(1, 0)
+
+    send_down(0)
+
+    near = jnp.minimum(z, n - 1 - z)
+    far_sign = jnp.where(z < n - 1 - z, 1, -1)
+
+    def owner_at(order):
+        close = order <= 2 * near
+        side = 2 * lax.rem(order + 1, 2) - 1
+        return z + jnp.where(close, side * ((order + 1) // 2), far_sign * (order - near))
+
+    def event(weight, number):
+        span = 2 * CHUNKS
+        close = number < near * span
+        rest = number - near * span
+        side = 2 * (number % 2) - 1
+        owner = z + jnp.where(
+            close,
+            side * (number // span + 1),
+            far_sign * (near + 1 + lax.div(jnp.maximum(rest, 0), CHUNKS)),
+        )
+        index = jnp.where(
+            close, (number % span) // 2, lax.rem(jnp.maximum(rest, 0), CHUNKS)
+        )
+        wait_piece(weight, owner, y, index)
+
+        @pl.when((owner < z) & (z < n - 1))
+        def _():
+            z_copy(weight, owner, index, 1).start()
+
+        @pl.when((owner > z) & (z > 0))
+        def _():
+            z_copy(weight, owner, index, 0).start()
+
+        y_copy(weight, owner, index).start()
+
+    total_events = (n - 1) * CHUNKS
+    done = [0, 0]
+
+    def pump(weight, until):
+        while done[weight] < min(until, total_events):
+            event(weight, done[weight])
+            done[weight] += 1
+            if weight == 0:
+                for stage in range(1, n - 1):
+                    if done[0] == min(stage * 2 * CHUNKS, total_events):
+                        send_down(stage)
+
+    @pl.when(z == 0)
+    def _():
+        k_buf[pl.ds(0, WINDOW), :] = jnp.zeros((WINDOW, HEAD_DIM), BF16)
+        v_buf[pl.ds(0, WINDOW), :] = jnp.zeros((WINDOW, HEAD_DIM), BF16)
+
+    for copy in locals_[:3]:
+        copy.wait()
+
+    @pl.when(z > 0)
+    def _():
+        tail_copy(0).wait_recv()
+        tail_copy(1).wait_recv()
+
+    heads = head_cols // HEAD_DIM
+    spread = jnp.where(
+        lax.broadcasted_iota(jnp.int32, (HEAD_DIM, head_cols), 1) % HEAD_DIM
+        == lax.broadcasted_iota(jnp.int32, (HEAD_DIM, head_cols), 0),
+        1.0,
+        0.0,
+    ).astype(BF16)
+    k_wide[...] = jnp.dot(k_buf[...], spread, preferred_element_type=F32).astype(BF16)
+    v_wide[...] = jnp.dot(v_buf[...], spread, preferred_element_type=F32).astype(BF16)
+
+    def attend(block, carry):
+        start = aligned(block, WINDOW)
+        q_rows = q_buf[pl.ds(start, WINDOW), :].astype(F32)
+        lane_head = lax.broadcasted_iota(jnp.int32, (WINDOW, head_cols), 1) // HEAD_DIM
+        stacked = jnp.concatenate(
+            [jnp.where(lane_head == h, q_rows, 0.0) for h in range(heads)], axis=0
+        ).astype(BF16)
+        scores = lax.dot_general(
+            stacked,
+            k_wide[pl.ds(start, 2 * WINDOW), :],
+            (((1,), (1,)), ((), ())),
+            preferred_element_type=F32,
+        ) * HEAD_DIM ** (-0.5)
+        i = lax.broadcasted_iota(jnp.int32, (heads * WINDOW, 2 * WINDOW), 0) % WINDOW
+        j = lax.broadcasted_iota(jnp.int32, (heads * WINDOW, 2 * WINDOW), 1)
+        first = WINDOW - z * rows - block * WINDOW
+        valid = (j > i) & (j <= i + WINDOW) & (j >= first)
+        scores = jnp.where(valid, scores, -1e30)
+        sinks = jnp.concatenate(
+            [jnp.full((WINDOW, 1), sink[h], F32) for h in range(heads)], axis=0
+        )
+        top = jnp.maximum(jnp.max(scores, axis=-1, keepdims=True), sinks)
+        weights = jnp.exp(scores - top)
+        total = jnp.sum(weights, axis=-1, keepdims=True) + jnp.exp(sinks - top)
+        probs = (weights / total).astype(BF16)
+        mixed_heads = jnp.dot(
+            probs, v_wide[pl.ds(start, 2 * WINDOW), :], preferred_element_type=F32
+        )
+        result = jnp.zeros((WINDOW, head_cols), F32)
+        for h in range(heads):
+            result += jnp.where(
+                lane_head == h, mixed_heads[h * WINDOW : (h + 1) * WINDOW], 0.0
+            )
+        attended[pl.ds(start, WINDOW), :] = result.astype(BF16)
+        return carry
+
+    blocks = rows // WINDOW
+    for block in range(0, blocks, 2):
+        lax.fori_loop(block, min(block + 2, blocks), attend, 0)
+        pump(0, block // 2 + 1)
+
+    def att_copy(step):
+        peer = lax.rem(me + step, 4)
+        return remote(
+            attended.at[pl.ds(aligned(peer, own), own), :],
+            att_all.at[me],
+            att_send.at[step - 1],
+            att_recv.at[me],
+            {"tp": peer},
+        )
+
+    def att_wait(step):
+        peer = lax.rem(me + step, 4)
+        remote(
+            att_all.at[peer], att_all.at[peer], att_send.at[step - 1], att_recv.at[peer], {"tp": peer}
+        ).wait_recv()
+
+    for step in (2, 1, 3):
+        att_copy(step).start()
+    att_all[me] = attended[pl.ds(aligned(me, own), own), :]
+    pump(0, 4)
+    locals_[3].wait()
+    locals_[4].wait()
+    for step in (1, 2, 3):
+        att_wait(step)
+
+    tile = 256
+
+    def project(index, squares):
+        span = pl.ds(aligned(index, tile), tile)
+        value = res_buf[:, span].astype(F32)
+        for peer in range(4):
+            value += jnp.dot(
+                att_all[peer],
+                ow_buf[peer * head_cols : (peer + 1) * head_cols, span],
+                preferred_element_type=F32,
+            )
+        value = value.astype(BF16).astype(F32)
+        mixed[:, span] = value
+        return squares + jnp.sum(value * value, axis=-1, keepdims=True)
+
+    squares = lax.fori_loop(0, wide // tile, project, jnp.zeros((own, 1), F32))
+    scale = lax.rsqrt(squares / wide + 1e-06)
+    own_rows = pl.ds(aligned(me, own), own)
+
+    def normalize(index, carry):
+        span = pl.ds(aligned(index, tile), tile)
+        normed[own_rows, span] = (mixed[:, span] * scale * gain[:, span]).astype(BF16)
+        return carry
+
+    lax.fori_loop(0, wide // tile, normalize, 0)
+
+    def norm_copy(slot, source, target):
+        place = normed.at[pl.ds(aligned(source, own), own), :]
+        return remote(place, place, norm_send.at[slot], norm_recv.at[source], {"tp": target})
+
+    norm_copy(0, me, across).start()
+    norm_copy(1, me, partner).start()
+    pump(0, 3 * total_events // 4)
+    norm_copy(2, across, across).wait_recv()
+    norm_copy(2, across, partner).start()
+    pump(0, total_events)
+
+    locals_[5].wait()
+    norm_copy(2, partner, partner).wait_recv()
+    norm_copy(2, diagonal, partner).wait_recv()
+
+    for order in range(n):
+        owner = owner_at(order) if order else z
+        if order:
+            for index in range(CHUNKS):
+                wait_piece(0, owner, 1 - y, index)
+
+        def up_step(index, carry, owner=owner, order=order):
+            span = pl.ds(aligned(index, tile), tile)
+            value = jnp.dot(
+                normed[:, pl.ds(aligned(owner, depth), depth)],
+                up_buf[pl.ds(aligned(owner, depth), depth), span],
+                preferred_element_type=F32,
+            )
+            if order:
+                value += acc[:, span]
+            if order == n - 1:
+                hidden[:, span] = jnp.square(jnp.maximum(value, 0.0)).astype(BF16)
+            else:
+                acc[:, span] = value
+            return carry
+
+        lax.fori_loop(0, cols // tile, up_step, 0)
+        if order == n - 2:
+            pump(1, CHUNKS)
+
+    def pair_copy(order, slot):
+        group = (partner, diagonal)[slot]
+        return remote(
+            terms.at[order, pl.ds(aligned(group, own), own), :],
+            pair_in.at[order, slot],
+            pair_send.at[order, slot],
+            pair_recv.at[order, slot],
+            {"tp": partner},
+        )
+
+    def peer_copy(order):
+        return remote(
+            chip_sum.at[order],
+            peer_in.at[order],
+            peer_send.at[order],
+            peer_recv.at[order],
+            {"tp": across},
+        )
+
+    def finish(order):
+        owner = owner_at(order) if order else z
+        span = pl.ds(aligned(owner, width), width)
+        peer_copy(order).wait_recv()
+        pair_copy(order, 0).wait_recv()
+        total = (
+            terms[order, own_rows, :].astype(F32)
+            + pair_in[order, 0].astype(F32)
+            + peer_in[order].astype(F32)
+        )
+        out[:, span] = (mixed[:, span] + total).astype(BF16)
+
+    locals_[6].wait()
+    for order in range(n):
+        owner = owner_at(order) if order else z
+        if order:
+            pump(1, (order + 1) * CHUNKS if order % 2 else order * CHUNKS)
+            for index in range(CHUNKS):
+                wait_piece(1, owner, 1 - y, index)
+
+        def down_step(index, carry, owner=owner, order=order):
+            span = pl.ds(aligned(index, tile), tile)
+            terms[order, :, span] = jnp.dot(
+                hidden[...], down_buf[owner, :, span], preferred_element_type=F32
+            ).astype(BF16)
+            return carry
+
+        lax.fori_loop(0, width // tile, down_step, 0)
+        pair_copy(order, 1).start()
+        pair_copy(order, 0).start()
+        pair_copy(order, 1).wait_recv()
+        other = pl.ds(aligned(across, own), own)
+        chip_sum[order] = (
+            terms[order, other, :].astype(F32) + pair_in[order, 1].astype(F32)
+        ).astype(BF16)
+        peer_copy(order).start()
+        if order:
+            finish(order - 1)
+    finish(n - 1)
+
+    for step in (1, 2, 3):
+        att_copy(step).wait_send()
+    norm_copy(0, me, across).wait_send()
+    norm_copy(1, me, partner).wait_send()
+    norm_copy(2, across, partner).wait_send()
+    for order in range(n):
+        pair_copy(order, 0).wait_send()
+        pair_copy(order, 1).wait_send()
+        peer_copy(order).wait_send()
+
+    @pl.when(z < n - 1)
+    def _():
+        tail_copy(0).wait_send()
+        tail_copy(1).wait_send()
+
+    for weight in range(2):
+        for owner in range(n):
+
+            @pl.when((z >= owner) & (z < n - 1))
+            def _():
+                for index in range(CHUNKS):
+                    z_copy(weight, owner, index, 1).wait_send()
+
+            @pl.when((z <= owner) & (z > 0))
+            def _():
+                for index in range(CHUNKS):
+                    z_copy(weight, owner, index, 0).wait_send()
+
+            @pl.when(z != owner)
+            def _():
+                for index in range(CHUNKS):
+                    y_copy(weight, owner, index).wait_send()
+
+
+def fused_body(
+    n,
+    queries,
+    key_rows,
+    value_rows,
+    sink_logits,
+    out_weight,
+    residual,
+    norm_gain,
+    up_weight,
+    down_weight,
+):
+    rows, head_cols = queries.shape
+    own, wide = residual.shape
+    depth, cols = up_weight.shape
+    width = down_weight.shape[1]
+    vmem = lambda *shape: pltpu.VMEM(shape, BF16)
+    dma = lambda *shape: pltpu.SemaphoreType.DMA(shape)
+    hbm = pl.BlockSpec(memory_space=pl.ANY)
+    return pl.pallas_call(
+        functools.partial(layer_kernel, n),
+        out_shape=jax.ShapeDtypeStruct((own, wide), BF16),
+        in_specs=[
+            hbm,
+            hbm,
+            hbm,
+            pl.BlockSpec(memory_space=pltpu.SMEM),
+            hbm,
+            hbm,
+            pl.BlockSpec(memory_space=pltpu.VMEM),
+            hbm,
+            hbm,
+        ],
+        out_specs=pl.BlockSpec(memory_space=pltpu.VMEM),
+        scratch_shapes=[
+            vmem(rows, head_cols),
+            vmem(rows + WINDOW, HEAD_DIM),
+            vmem(rows + WINDOW, HEAD_DIM),
+            vmem(rows + WINDOW, head_cols),
+            vmem(rows + WINDOW, head_cols),
+            vmem(rows, head_cols),
+            vmem(4, own, head_cols),
+            vmem(*out_weight.shape),
+            vmem(own, wide),
+            pltpu.VMEM((own, wide), F32),
+            vmem(rows, wide),
+            vmem(n * depth, cols),
+            vmem(n, cols, width),
+            pltpu.VMEM((rows, cols), F32),
+            vmem(rows, cols),
+            vmem(n, rows, width),
+            vmem(n, 2, own, width),
+            vmem(n, own, width),
+            vmem(n, own, width),
+            dma(7),
+            dma(2),
+            dma(2),
+            dma(2, 2, n, CHUNKS),
+            dma(2, n, CHUNKS),
+            dma(2, n, 2, CHUNKS),
+            dma(3),
+            dma(4),
+            dma(3),
+            dma(4),
+            dma(n, 2),
+            dma(n, 2),
+            dma(n),
+            dma(n),
+        ],
+        compiler_params=pltpu.CompilerParams(
+            collective_id=0, has_side_effects=True, vmem_limit_bytes=60 * 1024 * 1024
+        ),
+    )(
+        queries,
+        key_rows,
+        value_rows,
+        sink_logits,
+        out_weight,
+        residual,
+        norm_gain.reshape(1, -1),
+        up_weight,
+        down_weight,
+    )
+
+
 def solution(mesh):
     in_specs = (
         P(("grp", "sp"), "tp"),
@@ -110,4 +689,20 @@
         P("tp", "sp"),
     )
     out_specs = P(("grp", "sp", "tp"), None)
-    return jax.shard_map(body, mesh=mesh, in_specs=in_specs, out_specs=out_specs, check_vma=False)
+    n = mesh.shape["sp"]
+    shards_fit = 2 <= n <= 8
+
+    def layer(*arrays):
+        key_rows, up_weight, down_weight = arrays[1], arrays[7], arrays[8]
+        fits = (
+            shards_fit
+            and mesh.shape["grp"] == 2
+            and mesh.shape["tp"] == 4
+            and key_rows.shape[1] == HEAD_DIM
+            and up_weight.shape[0] % (32 * CHUNKS) == 0
+            and up_weight.shape[1] % 256 == 0
+            and down_weight.shape[1] % 256 == 0
+        )
+        return (functools.partial(fused_body, n) if fits else body)(*arrays)
+
+    return jax.shard_map(layer, mesh=mesh, in_specs=in_specs, out_specs=out_specs, check_vma=False)

time: 279 us -> 116 us (0.42)
  waiting for transfers between devices: 226 us -> 0 us
  Pallas kernels: 0 us -> 110 us
  matrix products: 17.5 us -> 0 us
  between operations: 15.2 us -> 0.01 us
  other arithmetic: 8.43 us -> 0 us
  starting transfers between devices: 5.11 us -> 0 us
    all_gather x3 -> x0, waiting for transfers between devices: 150 us -> none  [the longest x1 80.6 us: body(): lax.all_gather(down_weight, 'sp', axis=1, tiled=True)]
    pallas_call x0 -> x1, Pallas kernels: none -> 110 us  [fused_body(): pl.pallas_call(functools.partial(layer_kernel, n), out_shape=jax.ShapeDty...]
    reduce_scatter x2 -> x0, waiting for transfers between devices: 75.1 us -> none  [the longest x1 38 us: body(): lax.psum_scatter(terms.astype(jnp.bfloat16), 'tp', scatter_dimension=0, t...]
    dot_general x4 -> x0, matrix products: 17.5 us -> none  [the longest x1 11.9 us: body(): jnp.dot(hidden, lax.all_gather(down_weight, 'sp', axis=1, tiled=True), pr...]
    unnamed x8 -> x3, local copies, waits for them, and re-layouts: 0.02 us -> 5.5 us
    ppermute x1 -> x0, starting transfers between devices: 4.95 us -> none  [shifted(): lax.ppermute(value, axis, [(source, source + steps) for source in range(l...]
    convert_element_type x2 -> x0, other arithmetic: 4.72 us -> none  [the longest x1 2.4 us: body(): return (mixed32 + down).astype(jnp.bfloat16)]
    slice x11 -> x0, local copies, waits for them, and re-layouts: 3.82 us -> none  [the longest x4 1.19 us: band_attend(): value_blocks = jnp.concatenate([all_values[:-1], all_values[1:]], axis=1)]
  transfers between devices with their start and end apart: 6 -> 0, of which waited for: 5 -> 0; matrix products, arithmetic and copies ran while one was open for 3% -> 0% of each run, Pallas kernels for 0% -> 0%
where the time goes in v1:
time: 116 us; the launch traced here: 115 us
  Pallas kernels  110 us (95%)
  local copies, waits for them, and re-layouts  5.5 us (5%)
    pallas_call x1, Pallas kernels, fused_body(): pl.pallas_call(functools.partial(layer_kernel, n), out_shape=jax.ShapeDty...  110 us
    unnamed x3, local copies, waits for them, and re-layouts  5.5 us

profile of v1, /device:TPU:0, one launch (start us, length us, event | category | flops | bytes accessed | tf_op | source)
XLA Modules:
  0.0 115.4 jit_solution(2613186070509712014)
XLA Ops:
  0.0 1.7 %copy.10.keys = bf16[768,64]{1,0:T(8,128)(2,1)} copy(bf16[768,64]{0,1:T(8,128)(2,1)} %param.10) | data formatting | bytes 196608 | tf_op args[1]
  1.7 1.7 %copy.11.values = bf16[768,64]{1,0:T(8,128)(2,1)} copy(bf16[768,64]{0,1:T(8,128)(2,1)} %param.11) | data formatting | bytes 196608 | tf_op args[2]
  3.4 109.8 %shard_map.91 = bf16[192,2048]{1,0:T(8,128)(2,1)} custom-call(bf16[768,256]{1,0:T(8,128)(2,1)} %queries.1, bf16[768,64]{1,0:T(8,128)(2,1)} %copy.10.keys, bf16[768,64]{1,0:T(8,128)(2,1)} %copy.11.values, f32[4]{0:T(128)} %sink.1, bf16[1024,2048]{1,0:T(8,128)(2,1)} %out_weight.1, bf16[192,2048]{1,0:T(8,128)(2,1)} %residual.1, f32[1,2048]{1,0:T(1,128)} %bitcast.1, ...), custom_call_target="tpu_custom_call" | custom-call | tf_op jit(solution)/shard_map/pallas_call | solution.py:613
  113.3 2.1 %copy.13 = bf16[192,2048]{1,0:T(8,128)(2,1)} copy(bf16[192,2048]{1,0:T(8,128)(2,1)} %shard_map.91) | data formatting | bytes 1572864

commit v2 on v1

--- a/solution.py
+++ b/solution.py
@@ -102,6 +102,7 @@
 
 
 CHUNKS = 4
+LEAD = 2
 F32 = jnp.float32
 BF16 = jnp.bfloat16
 
@@ -179,7 +180,8 @@
     width = down.shape[1]
     cols = up.shape[1]
     wide = n * width
-    chunk = (depth // 2 // CHUNKS, down.shape[0] // 2 // CHUNKS)
+    part = width // 2
+    chunk = (depth // 2 // CHUNKS, down.shape[0] // 2 // (CHUNKS // 2))
 
     barrier = pltpu.get_barrier_semaphore()
     for step in range(1, 4):
@@ -207,13 +209,14 @@
 
     own_up = up_buf.at[pl.ds(aligned(z, depth), depth), :]
     locals_ = [
-        pltpu.make_async_copy(keys, k_buf.at[pl.ds(WINDOW, rows), :], local_sem.at[0]),
-        pltpu.make_async_copy(values, v_buf.at[pl.ds(WINDOW, rows), :], local_sem.at[1]),
+        pltpu.make_async_copy(keys, k_buf.at[:, pl.ds(WINDOW, rows)], local_sem.at[0]),
+        pltpu.make_async_copy(values, v_buf.at[:, pl.ds(WINDOW, rows)], local_sem.at[1]),
         pltpu.make_async_copy(queries, q_buf, local_sem.at[2]),
         pltpu.make_async_copy(out_weight, ow_buf, local_sem.at[3]),
         pltpu.make_async_copy(residual, res_buf, local_sem.at[4]),
         pltpu.make_async_copy(up, own_up, local_sem.at[5]),
-        pltpu.make_async_copy(down, down_buf.at[z], local_sem.at[6]),
+        pltpu.make_async_copy(down.at[:, pl.ds(0, part)], down_buf.at[z, 0], local_sem.at[6]),
+        pltpu.make_async_copy(down.at[:, pl.ds(part, part)], down_buf.at[z, 1], local_sem.at[7]),
     ]
     for copy in locals_:
         copy.start()
@@ -225,13 +228,20 @@
         if weight == 0:
             start = owner * depth + half * (depth // 2) + index * chunk[0]
             return up_buf.at[pl.ds(pl.multiple_of(start, chunk[0]), chunk[0]), :]
-        start = half * (CHUNKS * chunk[1]) + index * chunk[1]
-        return down_buf.at[owner, pl.ds(pl.multiple_of(start, chunk[1]), chunk[1]), :]
+        start = half * (2 * chunk[1]) + (index % 2) * chunk[1]
+        return down_buf.at[
+            owner, index // 2, pl.ds(pl.multiple_of(start, chunk[1]), chunk[1]), :
+        ]
 
     def own_piece(weight, index):
-        start = y * (CHUNKS * chunk[weight]) + index * chunk[weight]
-        ref = up if weight == 0 else down
-        return ref.at[pl.ds(pl.multiple_of(start, chunk[weight]), chunk[weight]), :]
+        if weight == 0:
+            start = y * (CHUNKS * chunk[0]) + index * chunk[0]
+            return up.at[pl.ds(pl.multiple_of(start, chunk[0]), chunk[0]), :]
+        start = y * (2 * chunk[1]) + (index % 2) * chunk[1]
+        return down.at[
+            pl.ds(pl.multiple_of(start, chunk[1]), chunk[1]),
+            pl.ds(index // 2 * (width // 2), width // 2),
+        ]
 
     def z_copy(weight, owner, index, upward, source=None):
         place = piece(weight, owner, y, index)
@@ -270,8 +280,8 @@
     def tail_copy(which):
         source, place = ((keys, k_buf), (values, v_buf))[which]
         return remote(
-            source.at[pl.ds(rows - WINDOW, WINDOW), :],
-            place.at[pl.ds(0, WINDOW), :],
+            source.at[:, pl.ds(rows - WINDOW, WINDOW)],
+            place.at[:, pl.ds(0, WINDOW)],
             tail_send.at[which],
             tail_recv.at[which],
             {"sp": z + 1},
@@ -306,7 +316,7 @@
         side = 2 * lax.rem(order + 1, 2) - 1
         return z + jnp.where(close, side * ((order + 1) // 2), far_sign * (order - near))
 
-    def event(weight, number):
+    def shard_at(number):
         span = 2 * CHUNKS
         close = number < near * span
         rest = number - near * span
@@ -319,6 +329,10 @@
         index = jnp.where(
             close, (number % span) // 2, lax.rem(jnp.maximum(rest, 0), CHUNKS)
         )
+        return owner, index
+
+    def event(weight, number):
+        owner, index = shard_at(number)
         wait_piece(weight, owner, y, index)
 
         @pl.when((owner < z) & (z < n - 1))
@@ -332,21 +346,30 @@
         y_copy(weight, owner, index).start()
 
     total_events = (n - 1) * CHUNKS
-    done = [0, 0]
-
-    def pump(weight, until):
-        while done[weight] < min(until, total_events):
-            event(weight, done[weight])
-            done[weight] += 1
-            if weight == 0:
-                for stage in range(1, n - 1):
-                    if done[0] == min(stage * 2 * CHUNKS, total_events):
-                        send_down(stage)
+    done = [0]
+    halves = [0]
+
+    def pump(until):
+        while done[0] < min(until, 2 * total_events):
+            weight, number = divmod(done[0], total_events)
+            event(weight, number)
+            done[0] += 1
+            for stage in range(1, n - 1):
+                if done[0] == min(stage * 2 * CHUNKS, total_events):
+                    send_down(stage)
+
+    def take_halves(until):
+        while halves[0] < until:
+            pump(halves[0] + 1 + LEAD)
+            weight, number = divmod(halves[0], total_events)
+            owner, index = shard_at(number)
+            wait_piece(weight, owner, 1 - y, index)
+            halves[0] += 1
 
     @pl.when(z == 0)
     def _():
-        k_buf[pl.ds(0, WINDOW), :] = jnp.zeros((WINDOW, HEAD_DIM), BF16)
-        v_buf[pl.ds(0, WINDOW), :] = jnp.zeros((WINDOW, HEAD_DIM), BF16)
+        k_buf[:, pl.ds(0, WINDOW)] = jnp.zeros((HEAD_DIM, WINDOW), BF16)
+        v_buf[:, pl.ds(0, WINDOW)] = jnp.zeros((HEAD_DIM, WINDOW), BF16)
 
     for copy in locals_[:3]:
         copy.wait()
@@ -357,14 +380,9 @@
         tail_copy(1).wait_recv()
 
     heads = head_cols // HEAD_DIM
-    spread = jnp.where(
-        lax.broadcasted_iota(jnp.int32, (HEAD_DIM, head_cols), 1) % HEAD_DIM
-        == lax.broadcasted_iota(jnp.int32, (HEAD_DIM, head_cols), 0),
-        1.0,
-        0.0,
-    ).astype(BF16)
-    k_wide[...] = jnp.dot(k_buf[...], spread, preferred_element_type=F32).astype(BF16)
-    v_wide[...] = jnp.dot(v_buf[...], spread, preferred_element_type=F32).astype(BF16)
+    for h in range(heads):
+        k_wide[h * HEAD_DIM : (h + 1) * HEAD_DIM, :] = k_buf[...]
+        v_wide[h * HEAD_DIM : (h + 1) * HEAD_DIM, :] = v_buf[...]
 
     def attend(block, carry):
         start = aligned(block, WINDOW)
@@ -373,11 +391,8 @@
         stacked = jnp.concatenate(
             [jnp.where(lane_head == h, q_rows, 0.0) for h in range(heads)], axis=0
         ).astype(BF16)
-        scores = lax.dot_general(
-            stacked,
-            k_wide[pl.ds(start, 2 * WINDOW), :],
-            (((1,), (1,)), ((), ())),
-            preferred_element_type=F32,
+        scores = jnp.dot(
+            stacked, k_wide[:, pl.ds(start, 2 * WINDOW)], preferred_element_type=F32
         ) * HEAD_DIM ** (-0.5)
         i = lax.broadcasted_iota(jnp.int32, (heads * WINDOW, 2 * WINDOW), 0) % WINDOW
         j = lax.broadcasted_iota(jnp.int32, (heads * WINDOW, 2 * WINDOW), 1)
@@ -391,8 +406,11 @@
         weights = jnp.exp(scores - top)
         total = jnp.sum(weights, axis=-1, keepdims=True) + jnp.exp(sinks - top)
         probs = (weights / total).astype(BF16)
-        mixed_heads = jnp.dot(
-            probs, v_wide[pl.ds(start, 2 * WINDOW), :], preferred_element_type=F32
+        mixed_heads = lax.dot_general(
+            probs,
+            v_wide[:, pl.ds(start, 2 * WINDOW)],
+            (((1,), (1,)), ((), ())),
+            preferred_element_type=F32,
         )
         result = jnp.zeros((WINDOW, head_cols), F32)
         for h in range(heads):
@@ -405,7 +423,8 @@
     blocks = rows // WINDOW
     for block in range(0, blocks, 2):
         lax.fori_loop(block, min(block + 2, blocks), attend, 0)
-        pump(0, block // 2 + 1)
+        if block + 2 < blocks:
+            pump(block // 2 + 1)
 
     def att_copy(step):
         peer = lax.rem(me + step, 4)
@@ -426,7 +445,7 @@
     for step in (2, 1, 3):
         att_copy(step).start()
     att_all[me] = attended[pl.ds(aligned(me, own), own), :]
-    pump(0, 4)
+    pump(4)
     locals_[3].wait()
     locals_[4].wait()
     for step in (1, 2, 3):
@@ -464,10 +483,9 @@
 
     norm_copy(0, me, across).start()
     norm_copy(1, me, partner).start()
-    pump(0, 3 * total_events // 4)
+    pump(total_events)
     norm_copy(2, across, across).wait_recv()
     norm_copy(2, across, partner).start()
-    pump(0, total_events)
 
     locals_[5].wait()
     norm_copy(2, partner, partner).wait_recv()
@@ -476,8 +494,7 @@
     for order in range(n):
         owner = owner_at(order) if order else z
         if order:
-            for index in range(CHUNKS):
-                wait_piece(0, owner, 1 - y, index)
+            take_halves(min(order + order % 2, n - 1) * CHUNKS)
 
         def up_step(index, carry, owner=owner, order=order):
             span = pl.ds(aligned(index, tile), tile)
@@ -495,77 +512,78 @@
             return carry
 
         lax.fori_loop(0, cols // tile, up_step, 0)
-        if order == n - 2:
-            pump(1, CHUNKS)
-
-    def pair_copy(order, slot):
+
+    pieces = [(order, slice(0, width)) for order in range(n - 1)]
+    pieces += [(n - 1, slice(0, part)), (n - 1, slice(part, width))]
+
+    def pair_copy(which, slot):
+        order, span = pieces[which]
         group = (partner, diagonal)[slot]
         return remote(
-            terms.at[order, pl.ds(aligned(group, own), own), :],
-            pair_in.at[order, slot],
-            pair_send.at[order, slot],
-            pair_recv.at[order, slot],
+            terms.at[order, pl.ds(aligned(group, own), own), span],
+            pair_in.at[order, slot, :, span],
+            pair_send.at[which, slot],
+            pair_recv.at[which, slot],
             {"tp": partner},
         )
 
-    def peer_copy(order):
+    def peer_copy(which):
+        order, span = pieces[which]
         return remote(
-            chip_sum.at[order],
-            peer_in.at[order],
-            peer_send.at[order],
-            peer_recv.at[order],
+            chip_sum.at[order, :, span],
+            peer_in.at[order, :, span],
+            peer_send.at[which],
+            peer_recv.at[which],
             {"tp": across},
         )
 
-    def finish(order):
+    def finish(which):
+        order, span = pieces[which]
         owner = owner_at(order) if order else z
-        span = pl.ds(aligned(owner, width), width)
-        peer_copy(order).wait_recv()
-        pair_copy(order, 0).wait_recv()
+        size = span.stop - span.start
+        target = pl.ds(pl.multiple_of(owner * width + span.start, size), size)
+        peer_copy(which).wait_recv()
+        pair_copy(which, 0).wait_recv()
         total = (
-            terms[order, own_rows, :].astype(F32)
-            + pair_in[order, 0].astype(F32)
-            + peer_in[order].astype(F32)
-        )
-        out[:, span] = (mixed[:, span] + total).astype(BF16)
+            terms[order, own_rows, span].astype(F32)
+            + pair_in[order, 0, :, span].astype(F32)
+            + peer_in[order, :, span].astype(F32)
+        )
+        out[:, target] = (mixed[:, target] + total).astype(BF16)
 
     locals_[6].wait()
-    for order in range(n):
+    locals_[7].wait()
+    for which, (order, span) in enumerate(pieces):
         owner = owner_at(order) if order else z
         if order:
-            pump(1, (order + 1) * CHUNKS if order % 2 else order * CHUNKS)
-            for index in range(CHUNKS):
-                wait_piece(1, owner, 1 - y, index)
-
-        def down_step(index, carry, owner=owner, order=order):
-            span = pl.ds(aligned(index, tile), tile)
-            terms[order, :, span] = jnp.dot(
-                hidden[...], down_buf[owner, :, span], preferred_element_type=F32
+            whole = min(order + order % 2, n - 1) * CHUNKS
+            last = order == n - 1 and span.stop < width
+            take_halves(total_events + whole - (CHUNKS // 2 if last and n % 2 == 0 else 0))
+        for index in range(span.start // part, span.stop // part):
+            terms[order, :, index * part : (index + 1) * part] = jnp.dot(
+                hidden[...], down_buf[owner, index], preferred_element_type=F32
             ).astype(BF16)
-            return carry
-
-        lax.fori_loop(0, width // tile, down_step, 0)
-        pair_copy(order, 1).start()
-        pair_copy(order, 0).start()
-        pair_copy(order, 1).wait_recv()
+        pair_copy(which, 1).start()
+        pair_copy(which, 0).start()
+        pair_copy(which, 1).wait_recv()
         other = pl.ds(aligned(across, own), own)
-        chip_sum[order] = (
-            terms[order, other, :].astype(F32) + pair_in[order, 1].astype(F32)
+        chip_sum[order, :, span] = (
+            terms[order, other, span].astype(F32) + pair_in[order, 1, :, span].astype(F32)
         ).astype(BF16)
-        peer_copy(order).start()
-        if order:
-            finish(order - 1)
-    finish(n - 1)
+        peer_copy(which).start()
+        if which:
+            finish(which - 1)
+    finish(len(pieces) - 1)
 
     for step in (1, 2, 3):
         att_copy(step).wait_send()
     norm_copy(0, me, across).wait_send()
     norm_copy(1, me, partner).wait_send()
     norm_copy(2, across, partner).wait_send()
-    for order in range(n):
-        pair_copy(order, 0).wait_send()
-        pair_copy(order, 1).wait_send()
-        peer_copy(order).wait_send()
+    for which in range(len(pieces)):
+        pair_copy(which, 0).wait_send()
+        pair_copy(which, 1).wait_send()
+        peer_copy(which).wait_send()
 
     @pl.when(z < n - 1)
     def _():
@@ -627,10 +645,10 @@
         out_specs=pl.BlockSpec(memory_space=pltpu.VMEM),
         scratch_shapes=[
             vmem(rows, head_cols),
-            vmem(rows + WINDOW, HEAD_DIM),
-            vmem(rows + WINDOW, HEAD_DIM),
-            vmem(rows + WINDOW, head_cols),
-            vmem(rows + WINDOW, head_cols),
+            vmem(HEAD_DIM, rows + WINDOW),
+            vmem(HEAD_DIM, rows + WINDOW),
+            vmem(head_cols, rows + WINDOW),
+            vmem(head_cols, rows + WINDOW),
             vmem(rows, head_cols),
             vmem(4, own, head_cols),
             vmem(*out_weight.shape),
@@ -638,14 +656,14 @@
             pltpu.VMEM((own, wide), F32),
             vmem(rows, wide),
             vmem(n * depth, cols),
-            vmem(n, cols, width),
+            vmem(n, 2, cols, width // 2),
             pltpu.VMEM((rows, cols), F32),
             vmem(rows, cols),
             vmem(n, rows, width),
             vmem(n, 2, own, width),
             vmem(n, own, width),
             vmem(n, own, width),
-            dma(7),
+            dma(8),
             dma(2),
             dma(2),
             dma(2, 2, n, CHUNKS),
@@ -655,18 +673,18 @@
             dma(4),
             dma(3),
             dma(4),
-            dma(n, 2),
-            dma(n, 2),
-            dma(n),
-            dma(n),
+            dma(n + 1, 2),
+            dma(n + 1, 2),
+            dma(n + 1),
+            dma(n + 1),
         ],
         compiler_params=pltpu.CompilerParams(
             collective_id=0, has_side_effects=True, vmem_limit_bytes=60 * 1024 * 1024
         ),
     )(
         queries,
-        key_rows,
-        value_rows,
+        key_rows.T,
+        value_rows.T,
         sink_logits,
         out_weight,
         residual,

time: 116 us -> 104 us (0.90)
  Pallas kernels: 110 us -> 102 us
  local copies, waits for them, and re-layouts: 5.5 us -> 2.09 us
    pallas_call x1, Pallas kernels: 110 us -> 102 us  [fused_body(): pl.pallas_call(functools.partial(layer_kernel, n), out_shape=jax.ShapeDty...]
    unnamed x3 -> x1, local copies, waits for them, and re-layouts: 5.5 us -> 2.09 us
where the time goes in v2:
time: 104 us
  Pallas kernels  102 us (98%)
  local copies, waits for them, and re-layouts  2.09 us (2%)
    pallas_call x1, Pallas kernels, fused_body(): pl.pallas_call(functools.partial(layer_kernel, n), out_shape=jax.ShapeDty...  102 us
    unnamed x1, local copies, waits for them, and re-layouts  2.09 us

profile of v2, /device:TPU:0, one launch (start us, length us, event | category | flops | bytes accessed | tf_op | source)
XLA Modules:
  0.0 104.1 jit_solution(15174155685834755888)
XLA Ops:
  0.0 102.0 %shard_map.91 = bf16[192,2048]{1,0:T(8,128)(2,1)} custom-call(bf16[768,256]{1,0:T(8,128)(2,1)} %queries.1, bf16[64,768]{1,0:T(8,128)(2,1)} %bitcast.3, bf16[64,768]{1,0:T(8,128)(2,1)} %bitcast.4, f32[4]{0:T(128)} %sink.1, bf16[1024,2048]{1,0:T(8,128)(2,1)} %out_weight.1, bf16[192,2048]{1,0:T(8,128)(2,1)} %residual.1, f32[1,2048]{1,0:T(1,128)} %bitcast.5, ...), custom_call_target="tpu_custom_call" | custom-call | tf_op jit(solution)/shard_map/pallas_call | solution.py:631
  102.0 2.1 %copy.11 = bf16[192,2048]{1,0:T(8,128)(2,1)} copy(bf16[192,2048]{1,0:T(8,128)(2,1)} %shard_map.91) | data formatting | bytes 1572864

commit v3 on v2

--- a/solution.py
+++ b/solution.py
@@ -102,7 +102,7 @@
 
 
 CHUNKS = 4
-LEAD = 2
+LEAD = 4
 F32 = jnp.float32
 BF16 = jnp.bfloat16
 
@@ -483,7 +483,7 @@
 
     norm_copy(0, me, across).start()
     norm_copy(1, me, partner).start()
-    pump(total_events)
+    pump(total_events + 2)
     norm_copy(2, across, across).wait_recv()
     norm_copy(2, across, partner).start()
 

time: 104 us -> 98.8 us (0.950)
  Pallas kernels: 102 us -> 96.5 us
    pallas_call x1, Pallas kernels: 102 us -> 96.5 us  [fused_body(): pl.pallas_call(functools.partial(layer_kernel, n), out_shape=jax.ShapeDty...]
where the time goes in v3:
time: 98.8 us; the launch traced here: 98.5 us
  Pallas kernels  96.5 us (98%)
  local copies, waits for them, and re-layouts  2.09 us (2%)
    pallas_call x1, Pallas kernels, fused_body(): pl.pallas_call(functools.partial(layer_kernel, n), out_shape=jax.ShapeDty...  96.5 us
    unnamed x1, local copies, waits for them, and re-layouts  2.09 us

profile of v3, /device:TPU:0, one launch (start us, length us, event | category | flops | bytes accessed | tf_op | source)
XLA Modules:
  0.0 98.5 jit_solution(574465042941195124)
XLA Ops:
  0.0 96.5 %shard_map.91 = bf16[192,2048]{1,0:T(8,128)(2,1)} custom-call(bf16[768,256]{1,0:T(8,128)(2,1)} %queries.1, bf16[64,768]{1,0:T(8,128)(2,1)} %bitcast.3, bf16[64,768]{1,0:T(8,128)(2,1)} %bitcast.4, f32[4]{0:T(128)} %sink.1, bf16[1024,2048]{1,0:T(8,128)(2,1)} %out_weight.1, bf16[192,2048]{1,0:T(8,128)(2,1)} %residual.1, f32[1,2048]{1,0:T(1,128)} %bitcast.5, ...), custom_call_target="tpu_custom_call" | custom-call | tf_op jit(solution)/shard_map/pallas_call | solution.py:631
  96.5 2.1 %copy.11 = bf16[192,2048]{1,0:T(8,128)(2,1)} copy(bf16[192,2048]{1,0:T(8,128)(2,1)} %shard_map.91) | data formatting | bytes 1572864
